TPU v7x, 32 devices: a whole 2x2x4 slice. The times are simulated.
32 devices in a mesh: sp: 16 (over z, y, x), tp: 2 (over core).
Axes of the slice: x: 2, y: 2, z: 4, core: 2. Of those that a mesh axis runs over, the one named last changes fastest.
Arguments:
- conv_value: bfloat16 [8192, 1536], P('sp', 'tp'), may hold values from -6 to 6
- conv_gate: bfloat16 [8192, 1536], P('sp', 'tp'), may hold values from -8 to 8
- conv_out: bfloat16 [8192, 1536], P('sp', 'tp'), may hold values from -40 to 40
- conv_taps: bfloat16 [31, 1536], P(None, 'tp'), may hold values from -1 to 1
- norm_gain: float32 [1536], P('tp'), may hold values from 0.1 to 1.9
- norm_shift: float32 [1536], P('tp'), may hold values from -3 to 3
- proj_weight: bfloat16 [2048, 1536], P(None, 'tp'), may hold values from -0.15625 to 0.15625
- out_grad: bfloat16 [8192, 2048], P('sp'), may hold values from -6 to 6
Outputs:
- grad_value: bfloat16 [8192, 1536], P('sp', 'tp')
- grad_gate: bfloat16 [8192, 1536], P('sp', 'tp')
- grad_taps: float32 [31, 1536], P(None, 'tp')
- grad_gain: float32 [1536], P('tp')
- grad_shift: float32 [1536], P('tp')
- grad_proj: float32 [2048, 1536], P('sp', 'tp')
All inputs are finite; a program needn't handle non-finite values.
Results may differ from a plain program's by a relative error of at most 0.005.
Values may be sent and summed in bfloat16 or wider, within the bound.
A program may use at most 64 MiB of HBM per device.

v0:
```python
import functools

import jax
import jax.numpy as jnp
from jax import lax
from jax.experimental import pallas as pl
from jax.experimental.pallas import tpu as pltpu
from jax.sharding import PartitionSpec as P

norm_eps = 1e-05
MESH = pl.DeviceIdType.MESH
F32 = jnp.float32
BF16 = jnp.bfloat16
LANES = 128


def repeat(start, stop, body, unroll):
    assert (stop - start) % unroll == 0

    def step(i, carry):
        for u in range(unroll):
            body(start + i * unroll + u, carry)
        return carry

    lax.fori_loop(0, (stop - start) // unroll, step, 0)


def bit(x, b):
    return lax.rem(x // (1 << b), 2)


def coordinate_bits(index, nbits):
    bits = [bit(index, b) for b in range(nbits)]
    if nbits >= 2:
        bits[nbits - 2] = lax.rem(bits[nbits - 2] + bits[nbits - 1], 2)
    return bits


def partner_of(me, b, nbits):
    def flip(x, c):
        return x + (1 << c) * (1 - 2 * bit(me, c))

    other = flip(me, b)
    if nbits >= 2 and b == nbits - 1:
        other = flip(other, b - 1)
    return other


def stage_orders(nbits, groups):
    body = list(range(max(nbits - 1, 1)))
    tail = list(range(len(body), nbits))
    return [body[g % len(body):] + body[: g % len(body)] + tail for g in range(groups)]


def kernel(
    dims,
    cv_hbm, cg_hbm, co_hbm, taps_ref, gain_ref, shift_ref, w_hbm, og_hbm,
    gv_hbm, gg_hbm, small_out, proj_out,
    cv, cg, co, w, og, ogt, active, normed, dsilu, scaled, hgx, gv, gg,
    st_a, st_b, st_d, pk_a, pk_b, pk_c, pk_d, tapf, acc, sendbuf, recvbuf, tapacc, rowacc, flat, parts, mine, whole,
    in_sem, out_sem, tp_send, tp_recv, halo_send, halo_recv,
    rs_send, rs_recv, a_send, a_recv, b_send, b_recv,
):
    n, nbits, groups, chan_total = dims
    rows, chan = co.shape
    width = og.shape[1]
    block = width // n
    gcols = chan // groups
    cblocks = chan // LANES
    ntaps = taps_ref.shape[0]
    reach = ntaps - 1
    halo = hgx.shape[1] - rows
    chunk = mine.shape[0]
    per = small_out.shape[0]
    me = lax.axis_index("sp")
    core = lax.axis_index("tp")
    other_core = 1 - core
    orders = stage_orders(nbits, groups)

    loads = [
        pltpu.make_async_copy(src, dst, in_sem.at[i])
        for i, (src, dst) in enumerate(
            ((co_hbm, co), (og_hbm, og), (w_hbm, w), (cg_hbm, cg), (cv_hbm, cv))
        )
    ]
    loads[0].start()

    barrier = pltpu.get_barrier_semaphore()

    def greet(i, carry):
        pl.semaphore_signal(
            barrier, inc=1, device_id=(lax.rem(me + i, n), core), device_id_type=MESH
        )
        return carry

    lax.fori_loop(1, n, greet, 0)
    pl.semaphore_signal(barrier, inc=1, device_id=(me, other_core), device_id_type=MESH)

    lane_low = lax.broadcasted_iota(jnp.int32, (1, LANES), 1) < LANES // 2

    gain = gain_ref[...].reshape(1, chan)
    shift = shift_ref[...].reshape(1, chan)
    nt = rows // LANES
    mid = LANES // 2

    def pack(dst):
        for t in range(nt):
            turned = st_a[t * LANES:(t + 1) * LANES, :].T
            dst[0, t:t + 1, :] = turned[:1, :]
            dst[1, t:t + 1, :] = turned[mid:mid + 1, :]

    def unpack(packed, dst):
        for t in range(nt):
            dst[t * LANES:(t + 1) * LANES, :] = jnp.broadcast_to(packed[t:t + 1, :], (LANES, LANES)).T

    def wide(x):
        return jnp.concatenate([x] * cblocks, axis=1)

    loads[0].wait()
    for copy in loads[1:]:
        copy.start()

    def stats(i, carry):
        at = pl.ds(pl.multiple_of(i * 64, 64), 64)
        h = co[at, :].astype(F32)
        mean = jnp.sum(h, axis=1, keepdims=True) / chan
        d = h - mean
        m2 = jnp.sum(d * d, axis=1, keepdims=True)
        st_a[at, :] = jnp.where(lane_low, mean, m2)
        return carry

    repeat(0, rows // 64, stats, 2)
    pack(pk_a)
    pl.semaphore_wait(barrier, n)
    swap_a = pltpu.make_async_remote_copy(
        src_ref=pk_a, dst_ref=pk_b, send_sem=tp_send.at[0], recv_sem=tp_recv.at[0],
        device_id=(me, other_core), device_id_type=MESH,
    )
    swap_a.start()

    loads[1].wait()
    mybits = coordinate_bits(me, nbits)
    sub = LANES // block

    def transpose(c, carry):
        t = og[:, pl.ds(pl.multiple_of(c * LANES, LANES), LANES)].T
        for s in range(sub):
            rbits = coordinate_bits(c * sub + s, nbits)
            piece = t[s * block:(s + 1) * block, :]
            for g in range(groups):
                place = 0
                for k, b in enumerate(orders[g]):
                    place = place + lax.rem(rbits[b] + mybits[b], 2) * (1 << (nbits - 1 - k))
                ogt[g, place] = piece
        return carry

    lax.fori_loop(0, width // LANES, transpose, 0)

    swap_a.wait()
    gap = pk_a[0] - pk_b[0]
    variance = (pk_a[1] + pk_b[1] + gap * gap * (0.5 * chan)) / chan_total
    unpack(0.5 * (pk_a[0] + pk_b[0]), st_b)
    unpack(lax.rsqrt(variance + norm_eps), st_d)

    def norm(i, carry):
        at = pl.ds(pl.multiple_of(i * 32, 32), 32)
        z = (co[at, :].astype(F32) - wide(st_b[at, :])) * wide(st_d[at, :])
        normed[at, :] = z
        x = z * gain + shift
        sig = jax.nn.sigmoid(x)
        active[at, :] = (x * sig).astype(BF16)
        dsilu[at, :] = sig * (1.0 + x * (1.0 - sig))
        return carry

    repeat(0, rows // 32, norm, 2)

    def stage_copy(g, k):
        count = n >> (k + 1)
        off = n - (n >> k)
        return pltpu.make_async_remote_copy(
            src_ref=sendbuf.at[g, pl.ds(off, count)],
            dst_ref=recvbuf.at[g, pl.ds(off, count)],
            send_sem=rs_send.at[g, k],
            recv_sem=rs_recv.at[g, k],
            device_id=(partner_of(me, orders[g][k], nbits), core),
            device_id_type=MESH,
        )

    unit = max(1, n // 4)

    def product(g, start):
        lhs = ogt[g, pl.ds(start, unit)].reshape(unit * block, rows)
        out = jnp.dot(lhs, active[:, g * gcols:(g + 1) * gcols], preferred_element_type=F32)
        return out.reshape(unit, block, gcols)

    for g in range(groups):

        def far(i, carry, g=g):
            sendbuf[g, pl.ds(i * unit, unit)] = product(g, n // 2 + i * unit).astype(BF16)
            return carry

        lax.fori_loop(0, n // 2 // unit, far, 0)
        stage_copy(g, 0).start()
    def stage(k):
        count = n >> (k + 1)
        off = n - (n >> k)
        for g in range(groups):
            stage_copy(g, k).wait_recv()
            if k + 1 < nbits:
                keep = count // 2

                def pass_on(i, carry, g=g):
                    sendbuf[g, off + count + i] = (
                        acc[g, keep + i] + recvbuf[g, off + keep + i].astype(F32)
                    ).astype(BF16)
                    return carry

                lax.fori_loop(0, count - keep, pass_on, 0)
                stage_copy(g, k + 1).start()
            else:
                keep = count

            def take(i, carry, g=g):
                acc[g, i] = acc[g, i] + recvbuf[g, off + i].astype(F32)
                return carry

            lax.fori_loop(0, keep, take, 0)

    loads[2].wait()
    rowacc[...] = jnp.zeros_like(rowacc)

    def act(i, carry):
        at = pl.ds(pl.multiple_of(i * 128, 128), 128)
        scaled[at, :] = jnp.dot(og[at, :], w[...], preferred_element_type=F32)
        return carry

    lax.fori_loop(0, rows // 128, act, 0)

    def grads(i, carry):
        at = pl.ds(pl.multiple_of(i * 32, 32), 32)
        z = normed[at, :]
        ng = scaled[at, :] * dsilu[at, :]
        ngz = ng * z
        rowacc[0] = rowacc[0] + jnp.sum(ngz.reshape(4, 8, chan), axis=0)
        rowacc[1] = rowacc[1] + jnp.sum(ng.reshape(4, 8, chan), axis=0)
        s = ng * gain
        scaled[at, :] = s
        total = jnp.sum(s, axis=1, keepdims=True)
        dot = jnp.sum(s * z, axis=1, keepdims=True)
        st_a[at, :] = jnp.where(lane_low, total, dot)
        return carry

    repeat(0, rows // 32, grads, 2)
    pack(pk_c)
    swap_b = pltpu.make_async_remote_copy(
        src_ref=pk_c, dst_ref=pk_d, send_sem=tp_send.at[1], recv_sem=tp_recv.at[1],
        device_id=(me, other_core), device_id_type=MESH,
    )
    swap_b.start()
    tapacc[...] = jnp.zeros_like(tapacc)
    for c in range(cblocks):
        tapf[c] = taps_ref[:, c * LANES:(c + 1) * LANES].astype(F32)
    flat[...] = jnp.zeros_like(flat)
    for g in range(groups):

        def near(i, carry, g=g):
            acc[g, pl.ds(i * unit, unit)] = product(g, i * unit)
            return carry

        lax.fori_loop(0, n // 2 // unit, near, 0)

    swap_b.wait()
    unpack((pk_c[0] + pk_d[0]) / chan_total, st_a)
    unpack((pk_c[1] + pk_d[1]) / chan_total, st_b)

    def height(i, carry):
        at = pl.ds(pl.multiple_of(i * 32, 32), 32)
        hg = wide(st_d[at, :]) * (
            scaled[at, :] - wide(st_a[at, :]) - normed[at, :] * wide(st_b[at, :])
        )
        for c in range(cblocks):
            hgx[c, at, :] = hg[:, c * LANES:(c + 1) * LANES]
        return carry

    height(0, 0)
    halo_copy = pltpu.make_async_remote_copy(
        src_ref=hgx.at[:, pl.ds(0, halo)],
        dst_ref=hgx.at[:, pl.ds(rows, halo)],
        send_sem=halo_send, recv_sem=halo_recv,
        device_id=(lax.rem(me + n - 1, n), core), device_id_type=MESH,
    )

    @pl.when(me > 0)
    def _():
        halo_copy.start()

    repeat(1, rows // 32, height, 3)

    @pl.when(me == n - 1)
    def _():
        hgx[:, rows:, :] = jnp.zeros((cblocks, halo, LANES), F32)

    loads[3].wait()
    loads[4].wait()
    stage(0)

    @pl.when(me < n - 1)
    def _():
        halo_copy.wait_recv()

    step = 64
    steps = rows // step

    def conv(i, carry):
        c = i // steps
        r = pl.multiple_of(lax.rem(i, steps) * step, step)
        at = pl.ds(r, step)
        cols = pl.ds(pl.multiple_of(c * LANES, LANES), LANES)
        sig = jax.nn.sigmoid(cg[at, cols].astype(F32))
        value = cv[at, cols].astype(F32)
        gated = (value * sig).astype(BF16).astype(F32)
        total = jnp.zeros((step, LANES), F32)
        for j in range(ntaps):
            h = hgx[c, pl.ds(r + reach - j, step), :]
            total = total + tapf[c, pl.ds(j, 1), :] * h
            tapacc[c, j] = tapacc[c, j] + jnp.sum((gated * h).reshape(step // 8, 8, LANES), axis=0)
        gv[at, cols] = (total * sig).astype(BF16)
        gg[at, cols] = (total * value * sig * (1.0 - sig)).astype(BF16)
        return carry

    cut = cblocks * steps * 3 // 4
    lax.fori_loop(0, cut, conv, 0)
    stage(1)
    lax.fori_loop(cut, cblocks * steps, conv, 0)

    stores = [
        pltpu.make_async_copy(src, dst, out_sem.at[i])
        for i, (src, dst) in enumerate(((gv, gv_hbm), (gg, gg_hbm)))
    ]
    for copy in stores:
        copy.start()

    for c in range(cblocks):
        rowsum = jnp.sum(tapacc[c], axis=1)
        flat[c * per:c * per + ntaps, :] = rowsum
        for j in range(2):
            flat[c * per + ntaps + j:c * per + ntaps + j + 1, :] = jnp.sum(
                rowacc[j, :, c * LANES:(c + 1) * LANES], axis=0, keepdims=True
            )

    def spread(i):
        peer = lax.rem(me + i, n)
        return pltpu.make_async_remote_copy(
            src_ref=flat.at[pl.ds(pl.multiple_of(peer * chunk, chunk), chunk)],
            dst_ref=parts.at[me],
            send_sem=a_send.at[peer], recv_sem=a_recv.at[me],
            device_id=(peer, core), device_id_type=MESH,
        )

    def collect(i):
        peer = lax.rem(me + i, n)
        return pltpu.make_async_remote_copy(
            src_ref=mine,
            dst_ref=whole.at[pl.ds(pl.multiple_of(me * chunk, chunk), chunk)],
            send_sem=b_send.at[peer], recv_sem=b_recv.at[me],
            device_id=(peer, core), device_id_type=MESH,
        )

    def arrived_part(peer):
        return pltpu.make_async_remote_copy(
            src_ref=flat.at[pl.ds(pl.multiple_of(peer * chunk, chunk), chunk)],
            dst_ref=parts.at[peer],
            send_sem=a_send.at[peer], recv_sem=a_recv.at[peer],
            device_id=(peer, core), device_id_type=MESH,
        )

    def arrived_whole(peer):
        return pltpu.make_async_remote_copy(
            src_ref=mine,
            dst_ref=whole.at[pl.ds(pl.multiple_of(peer * chunk, chunk), chunk)],
            send_sem=b_send.at[peer], recv_sem=b_recv.at[peer],
            device_id=(peer, core), device_id_type=MESH,
        )

    def loop(body):
        def run(i, carry):
            body(i)
            return carry

        lax.fori_loop(1, n, run, 0)

    loop(lambda i: spread(i).start())
    mine[...] = flat[pl.ds(pl.multiple_of(me * chunk, chunk), chunk), :]

    for k in range(2, nbits - 1):
        stage(k)

    def add_part(i):
        peer = lax.rem(me + i, n)
        arrived_part(peer).wait_recv()
        mine[...] = mine[...] + parts[peer]

    loop(add_part)
    loop(lambda i: collect(i).start())
    whole[pl.ds(pl.multiple_of(me * chunk, chunk), chunk), :] = mine[...]

    stage(nbits - 1)
    for g in range(groups):
        proj_out[:, g * gcols:(g + 1) * gcols] = acc[g, 0]
    loop(lambda i: arrived_whole(lax.rem(me + i, n)).wait_recv())
    for c in range(cblocks):
        small_out[:, c * LANES:(c + 1) * LANES] = whole[c * per:(c + 1) * per, :]

    loop(lambda i: arrived_part(lax.rem(me + i, n)).wait_send())
    loop(lambda i: arrived_whole(lax.rem(me + i, n)).wait_send())
    for g in range(groups):
        for k in range(nbits):
            stage_copy(g, k).wait_send()

    @pl.when(me > 0)
    def _():
        halo_copy.wait_send()

    for copy in stores:
        copy.wait()


def place(gv_in, gg_in, small, proj_in, gv_out, gg_out, taps, gain, shift, proj_out, gv, gg, proj, in_sem, out_sem):
    ins = [
        pltpu.make_async_copy(src, dst, in_sem.at[i])
        for i, (src, dst) in enumerate(((gv_in, gv), (gg_in, gg), (proj_in, proj)))
    ]
    outs = [
        pltpu.make_async_copy(src, dst, out_sem.at[i])
        for i, (src, dst) in enumerate(((gv, gv_out), (gg, gg_out), (proj, proj_out)))
    ]
    for copy in ins:
        copy.start()
    ntaps = taps.shape[0]
    taps[...] = small[:ntaps, :]
    gain[...] = small[ntaps, :]
    shift[...] = small[ntaps + 1, :]
    for came, goes in zip(ins, outs):
        came.wait()
        goes.start()
    for copy in outs:
        copy.wait()


def local(conv_value, conv_gate, conv_out, conv_taps, norm_gain, norm_shift, proj_weight, out_grad):
    rows, chan = conv_value.shape
    ntaps = conv_taps.shape[0]
    width = out_grad.shape[1]
    n = lax.axis_size("sp")
    nbits = n.bit_length() - 1
    assert 1 << nbits == n and lax.axis_size("tp") == 2
    groups = 3
    gcols = chan // groups
    block = width // n
    cblocks = chan // LANES
    halo = 32
    per = -(-(ntaps + 2) // 8) * 8
    chunk = -(-(-(-per * cblocks // n)) // 8) * 8
    dims = (n, nbits, groups, chan * 2)
    hbm = pl.BlockSpec(memory_space=pl.ANY)
    vmem = pl.BlockSpec(memory_space=pltpu.VMEM)
    dma = pltpu.SemaphoreType.DMA
    grad_value, grad_gate, small, grad_proj = pl.pallas_call(
        functools.partial(kernel, dims),
        out_shape=(
            jax.ShapeDtypeStruct((rows, chan), BF16),
            jax.ShapeDtypeStruct((rows, chan), BF16),
            jax.ShapeDtypeStruct((per, chan), F32),
            jax.ShapeDtypeStruct((block, chan), F32),
        ),
        in_specs=[hbm, hbm, hbm, vmem, vmem, vmem, hbm, hbm],
        out_specs=(hbm, hbm, vmem, vmem),
        scratch_shapes=[
            pltpu.VMEM((rows, chan), BF16),
            pltpu.VMEM((rows, chan), BF16),
            pltpu.VMEM((rows, chan), BF16),
            pltpu.VMEM((width, chan), BF16),
            pltpu.VMEM((rows, width), BF16),
            pltpu.VMEM((groups, n, block, rows), BF16),
            pltpu.VMEM((rows, chan), BF16),
            pltpu.VMEM((rows, chan), F32),
            pltpu.VMEM((rows, chan), F32),
            pltpu.VMEM((rows, chan), F32),
            pltpu.VMEM((cblocks, rows + halo, LANES), F32),
            pltpu.VMEM((rows, chan), BF16),
            pltpu.VMEM((rows, chan), BF16),
            pltpu.VMEM((rows, LANES), F32),
            pltpu.VMEM((rows, LANES), F32),
            pltpu.VMEM((rows, LANES), F32),
            *[pltpu.VMEM((2, rows // LANES, LANES), F32)] * 4,
            pltpu.VMEM((cblocks, ntaps, LANES), F32),
            pltpu.VMEM((groups, n // 2, block, gcols), F32),
            pltpu.VMEM((groups, n, block, gcols), BF16),
            pltpu.VMEM((groups, n, block, gcols), BF16),
            pltpu.VMEM((cblocks, ntaps, 8, LANES), F32),
            pltpu.VMEM((2, 8, chan), F32),
            pltpu.VMEM((n * chunk, LANES), F32),
            pltpu.VMEM((n, chunk, LANES), F32),
            pltpu.VMEM((chunk, LANES), F32),
            pltpu.VMEM((n * chunk, LANES), F32),
            dma((5,)), dma((2,)),
            dma((2,)), dma((2,)),
            dma, dma,
            dma((groups, nbits)), dma((groups, nbits)),
            dma((n,)), dma((n,)),
            dma((n,)), dma((n,)),
        ],
        compiler_params=pltpu.CompilerParams(
            collective_id=0, has_side_effects=True, vmem_limit_bytes=60 * 1024 * 1024
        ),
    )(
        conv_value, conv_gate, conv_out, conv_taps, norm_gain, norm_shift, proj_weight, out_grad,
    )
    return pl.pallas_call(
        place,
        out_shape=(
            jax.ShapeDtypeStruct((rows, chan), BF16),
            jax.ShapeDtypeStruct((rows, chan), BF16),
            jax.ShapeDtypeStruct((ntaps, chan), F32),
            jax.ShapeDtypeStruct((chan,), F32),
            jax.ShapeDtypeStruct((chan,), F32),
            jax.ShapeDtypeStruct((block, chan), F32),
        ),
        in_specs=[hbm, hbm, vmem, hbm],
        out_specs=(hbm, hbm, vmem, vmem, vmem, hbm),
        scratch_shapes=[
            pltpu.VMEM((rows, chan), BF16),
            pltpu.VMEM((rows, chan), BF16),
            pltpu.VMEM((block, chan), F32),
            dma((3,)), dma((3,)),
        ],
    )(grad_value, grad_gate, small, grad_proj)


def solution(mesh):
    in_specs = (
        P("sp", "tp"),
        P("sp", "tp"),
        P("sp", "tp"),
        P(None, "tp"),
        P("tp"),
        P("tp"),
        P(None, "tp"),
        P("sp", None),
    )
    out_specs = (P("sp", "tp"), P("sp", "tp"), P(None, "tp"), P("tp"), P("tp"), P("sp", "tp"))
    return jax.shard_map(local, mesh=mesh, in_specs=in_specs, out_specs=out_specs, check_vma=False)
```

profile of v0, /device:TPU:0, one launch (start us, length us, event | category | flops | bytes accessed | tf_op | source)
XLA Modules:
  0.0 57.0 jit_solution(16691659044328701093)
XLA Ops:
  0.6 52.4 %shard_map.127 = (bf16[512,768]{1,0:T(8,128)(2,1)}, bf16[512,768]{1,0:T(8,128)(2,1)}, f32[40,768]{1,0:T(8,128)}, f32[128,768]{1,0:T(8,128)}) custom-call(bf16[512,768]{1,0:T(8,128)(2,1)} %cv_hbm.1, bf16[512,768]{1,0:T(8,128)(2,1)} %cg_hbm.1, bf16[512,768]{1,0:T(8,128)(2,1)} %co_hbm.1, bf16[31,768]{1,0:T(8,128)(2,1)} %taps_ref.1, f32[768]{0:T(1024)} %gain_ref.1, ...), custom_call_target="tpu_custom_call" | custom-call | tf_op jit(solution)/shard_map/pallas_call | solution.py:468
  53.0 4.0 %shard_map.128 = (bf16[512,768]{1,0:T(8,128)(2,1)}, bf16[512,768]{1,0:T(8,128)(2,1)}, f32[31,768]{1,0:T(8,128)}, f32[768]{0:T(1024)}, f32[768]{0:T(1024)}, /*index=5*/f32[128,768]{1,0:T(8,128)}) custom-call(bf16[512,768]{1,0:T(8,128)(2,1)} %get-tuple-element.10.gv_in, bf16[512,768]{1,0:T(8,128)(2,1)} %get-tuple-element.11.gg_in, ...), custom_call_target="tpu_custom_call" | custom-call | tf_op jit(solution)/shard_map/pallas_call | solution.py:519
where the time goes:
time: 57.3 us; the launch traced here: 57 us
  Pallas kernels  56.4 us (98%)
  between operations  0.64 us (1%)
    pallas_call x1, Pallas kernels, local(): pl.pallas_call(functools.partial(kernel, dims), out_shape=(jax.ShapeDtype...  52.4 us
    pallas_call x1, Pallas kernels, local(): pl.pallas_call(place, out_shape=(jax.ShapeDtypeStruct((rows, chan), BF16)...  4 us

commit v1 on v0

--- a/solution.py
+++ b/solution.py
@@ -55,10 +55,10 @@
 def kernel(
     dims,
     cv_hbm, cg_hbm, co_hbm, taps_ref, gain_ref, shift_ref, w_hbm, og_hbm,
-    gv_hbm, gg_hbm, small_out, proj_out,
-    cv, cg, co, w, og, ogt, active, normed, dsilu, scaled, hgx, gv, gg,
+    gv, gg, taps_out, gain_out, shift_out, proj_out,
+    cv, cg, co, w, og, ogt, active, normed, dsilu, scaled, hgx,
     st_a, st_b, st_d, pk_a, pk_b, pk_c, pk_d, tapf, acc, sendbuf, recvbuf, tapacc, rowacc, flat, parts, mine, whole,
-    in_sem, out_sem, tp_send, tp_recv, halo_send, halo_recv,
+    in_sem, tp_send, tp_recv, halo_send, halo_recv,
     rs_send, rs_recv, a_send, a_recv, b_send, b_recv,
 ):
     n, nbits, groups, chan_total = dims
@@ -71,7 +71,7 @@
     reach = ntaps - 1
     halo = hgx.shape[1] - rows
     chunk = mine.shape[0]
-    per = small_out.shape[0]
+    per = -(-(ntaps + 2) // 8) * 8
     me = lax.axis_index("sp")
     core = lax.axis_index("tp")
     other_core = 1 - core
@@ -333,13 +333,6 @@
     stage(1)
     lax.fori_loop(cut, cblocks * steps, conv, 0)
 
-    stores = [
-        pltpu.make_async_copy(src, dst, out_sem.at[i])
-        for i, (src, dst) in enumerate(((gv, gv_hbm), (gg, gg_hbm)))
-    ]
-    for copy in stores:
-        copy.start()
-
     for c in range(cblocks):
         rowsum = jnp.sum(tapacc[c], axis=1)
         flat[c * per:c * per + ntaps, :] = rowsum
@@ -409,7 +402,10 @@
         proj_out[:, g * gcols:(g + 1) * gcols] = acc[g, 0]
     loop(lambda i: arrived_whole(lax.rem(me + i, n)).wait_recv())
     for c in range(cblocks):
-        small_out[:, c * LANES:(c + 1) * LANES] = whole[c * per:(c + 1) * per, :]
+        cols = slice(c * LANES, (c + 1) * LANES)
+        taps_out[:, cols] = whole[c * per:c * per + ntaps, :]
+        gain_out[cols] = whole[c * per + ntaps, :]
+        shift_out[cols] = whole[c * per + ntaps + 1, :]
 
     loop(lambda i: arrived_part(lax.rem(me + i, n)).wait_send())
     loop(lambda i: arrived_whole(lax.rem(me + i, n)).wait_send())
@@ -421,29 +417,17 @@
     def _():
         halo_copy.wait_send()
 
-    for copy in stores:
-        copy.wait()
-
-
-def place(gv_in, gg_in, small, proj_in, gv_out, gg_out, taps, gain, shift, proj_out, gv, gg, proj, in_sem, out_sem):
-    ins = [
-        pltpu.make_async_copy(src, dst, in_sem.at[i])
-        for i, (src, dst) in enumerate(((gv_in, gv), (gg_in, gg), (proj_in, proj)))
+
+def place(*refs):
+    count = (len(refs) - 1) // 2
+    sem = refs[-1]
+    copies = [
+        pltpu.make_async_copy(src, dst, sem.at[i])
+        for i, (src, dst) in enumerate(zip(refs[:count], refs[count:-1]))
     ]
-    outs = [
-        pltpu.make_async_copy(src, dst, out_sem.at[i])
-        for i, (src, dst) in enumerate(((gv, gv_out), (gg, gg_out), (proj, proj_out)))
-    ]
-    for copy in ins:
+    for copy in copies:
         copy.start()
-    ntaps = taps.shape[0]
-    taps[...] = small[:ntaps, :]
-    gain[...] = small[ntaps, :]
-    shift[...] = small[ntaps + 1, :]
-    for came, goes in zip(ins, outs):
-        came.wait()
-        goes.start()
-    for copy in outs:
+    for copy in copies:
         copy.wait()
 
 
@@ -465,16 +449,18 @@
     hbm = pl.BlockSpec(memory_space=pl.ANY)
     vmem = pl.BlockSpec(memory_space=pltpu.VMEM)
     dma = pltpu.SemaphoreType.DMA
-    grad_value, grad_gate, small, grad_proj = pl.pallas_call(
+    results = pl.pallas_call(
         functools.partial(kernel, dims),
         out_shape=(
-            jax.ShapeDtypeStruct((rows, chan), BF16),
-            jax.ShapeDtypeStruct((rows, chan), BF16),
-            jax.ShapeDtypeStruct((per, chan), F32),
-            jax.ShapeDtypeStruct((block, chan), F32),
+            pltpu.VMEM((rows, chan), BF16),
+            pltpu.VMEM((rows, chan), BF16),
+            pltpu.VMEM((ntaps, chan), F32),
+            pltpu.VMEM((chan,), F32),
+            pltpu.VMEM((chan,), F32),
+            pltpu.VMEM((block, chan), F32),
         ),
         in_specs=[hbm, hbm, hbm, vmem, vmem, vmem, hbm, hbm],
-        out_specs=(hbm, hbm, vmem, vmem),
+        out_specs=(vmem,) * 6,
         scratch_shapes=[
             pltpu.VMEM((rows, chan), BF16),
             pltpu.VMEM((rows, chan), BF16),
@@ -487,8 +473,6 @@
             pltpu.VMEM((rows, chan), F32),
             pltpu.VMEM((rows, chan), F32),
             pltpu.VMEM((cblocks, rows + halo, LANES), F32),
-            pltpu.VMEM((rows, chan), BF16),
-            pltpu.VMEM((rows, chan), BF16),
             pltpu.VMEM((rows, LANES), F32),
             pltpu.VMEM((rows, LANES), F32),
             pltpu.VMEM((rows, LANES), F32),
@@ -503,7 +487,7 @@
             pltpu.VMEM((n, chunk, LANES), F32),
             pltpu.VMEM((chunk, LANES), F32),
             pltpu.VMEM((n * chunk, LANES), F32),
-            dma((5,)), dma((2,)),
+            dma((5,)),
             dma((2,)), dma((2,)),
             dma, dma,
             dma((groups, nbits)), dma((groups, nbits)),
@@ -518,23 +502,11 @@
     )
     return pl.pallas_call(
         place,
-        out_shape=(
-            jax.ShapeDtypeStruct((rows, chan), BF16),
-            jax.ShapeDtypeStruct((rows, chan), BF16),
-            jax.ShapeDtypeStruct((ntaps, chan), F32),
-            jax.ShapeDtypeStruct((chan,), F32),
-            jax.ShapeDtypeStruct((chan,), F32),
-            jax.ShapeDtypeStruct((block, chan), F32),
-        ),
-        in_specs=[hbm, hbm, vmem, hbm],
-        out_specs=(hbm, hbm, vmem, vmem, vmem, hbm),
-        scratch_shapes=[
-            pltpu.VMEM((rows, chan), BF16),
-            pltpu.VMEM((rows, chan), BF16),
-            pltpu.VMEM((block, chan), F32),
-            dma((3,)), dma((3,)),
-        ],
-    )(grad_value, grad_gate, small, grad_proj)
+        out_shape=tuple(jax.ShapeDtypeStruct(x.shape, x.dtype) for x in results),
+        in_specs=[vmem] * len(results),
+        out_specs=(hbm,) * len(results),
+        scratch_shapes=[dma((len(results),))],
+    )(*[pltpu.with_memory_space_constraint(x, pltpu.VMEM) for x in results])
 
 
 def solution(mesh):

time: 57.3 us -> 53.8 us (0.939)
  Pallas kernels: 56.4 us -> 52.9 us
    pallas_call x2, Pallas kernels: 56.4 us -> 52.9 us  [the longest x1 51.6 us: local(): pl.pallas_call(functools.partial(kernel, dims), out_shape=(pltpu.VMEM((ro...]
where the time goes in v1:
time: 53.8 us; the launch traced here: 53.6 us
  Pallas kernels  52.9 us (98%)
  between operations  0.64 us (1%)
    pallas_call x1, Pallas kernels, local(): pl.pallas_call(functools.partial(kernel, dims), out_shape=(pltpu.VMEM((ro...  51.6 us
    pallas_call x1, Pallas kernels, local(): pl.pallas_call(place, out_shape=tuple((jax.ShapeDtypeStruct(x.shape, x.dt...  1.36 us

profile of v1, /device:TPU:0, one launch (start us, length us, event | category | flops | bytes accessed | tf_op | source)
XLA Modules:
  0.0 53.6 jit_solution(13977955703863410051)
XLA Ops:
  0.6 51.6 %shard_map.127 = (bf16[512,768]{1,0:T(8,128)(2,1)S(1)}, bf16[512,768]{1,0:T(8,128)(2,1)S(1)}, f32[31,768]{1,0:T(8,128)S(1)}, f32[768]{0:T(1024)S(1)}, f32[768]{0:T(1024)S(1)}, /*index=5*/f32[128,768]{1,0:T(8,128)S(1)}) custom-call(bf16[512,768]{1,0:T(8,128)(2,1)} %cv_hbm.1, bf16[512,768]{1,0:T(8,128)(2,1)} %cg_hbm.1, bf16[512,768]{1,0:T(8,128)(2,1)} %co_hbm.1, ...), custom_call_target="tpu_custom_call" | custom-call | tf_op jit(solution)/shard_map/pallas_call | solution.py:452
  52.2 1.4 %shard_map.128 = (bf16[512,768]{1,0:T(8,128)(2,1)}, bf16[512,768]{1,0:T(8,128)(2,1)}, f32[31,768]{1,0:T(8,128)}, f32[768]{0:T(1024)}, f32[768]{0:T(1024)}, /*index=5*/f32[128,768]{1,0:T(8,128)}) custom-call(bf16[512,768]{1,0:T(8,128)(2,1)S(1)} %get-tuple-element.12.refs_0_, bf16[512,768]{1,0:T(8,128)(2,1)S(1)} %get-tuple-element.13.refs_1_, ...), custom_call_target="tpu_custom_call" | custom-call | tf_op jit(solution)/shard_map/pallas_call | solution.py:503

commit v2 on v1

v2 whole, which is shorter than its diff:
```python
import functools

import jax
import jax.numpy as jnp
from jax import lax
from jax.experimental import pallas as pl
from jax.experimental.pallas import tpu as pltpu
from jax.sharding import PartitionSpec as P

norm_eps = 1e-05
MESH = pl.DeviceIdType.MESH
F32 = jnp.float32
BF16 = jnp.bfloat16
LANES = 128
HALVES = 4
UNIT = 256
TAP_CUTS = 6
CONV_CUTS = 6
ORDERS = ('ybax', 'xbya', 'byxa', 'xaby', 'xbya', 'xayb', 'yxab', 'ybxa', 'yxba', 'axyb', 'yxab', 'ayxb')
PLAN = [
    ("far", 0), ("send", 0), ("send", 2), ("send", 3), ("far", 1), ("send", 5), ("send", 7), ("far", 2), ("send", 8),
    ("send", 11), ("act", 0), ("act", 1), ("act", 2), ("send", 4), ("send", 6), ("send", 9), ("act", 3), ("grads", 0),
    ("near", 0), ("near", 1), (0, 0), (3, 0), ("near", 2), ("height", 0), ("send", 1), ("send", 10), ("taps", 0),
    ("taps", 1), (5, 0), (7, 0), (11, 0), ("taps", 2), (2, 0), ("taps", 3), ("taps", 4), ("taps", 5), (4, 0), (8, 0),
    (9, 0), ("conv", 0), ("conv", 1), (0, 1), ("edge", 0), (3, 1), (6, 0), ("spread", 0), ("conv", 2), (1, 0), (5, 1),
    ("conv", 3), (8, 1), ("conv", 4), (10, 0), ("conv", 5), (7, 1), (9, 1), (11, 1), ("cedge", 0), (0, 2), (4, 1),
    (6, 1), (2, 1), (3, 2), (5, 2), (10, 1), (9, 2), (7, 2), (4, 2), (11, 2), (3, 3), (1, 1), ("collect", 0), (0, 3),
    (6, 2), (2, 2), (8, 2), (10, 2), (5, 3), (7, 3), (4, 3), (9, 3), (1, 2), (11, 3), (2, 3), (8, 3), (6, 3), (1, 3),
    (10, 3),
]


def repeat(start, stop, body, unroll):
    assert (stop - start) % unroll == 0

    def step(i, carry):
        for u in range(unroll):
            body(start + i * unroll + u, carry)
        return carry

    lax.fori_loop(0, (stop - start) // unroll, step, 0)


def bit(x, b):
    return lax.rem(x // (1 << b), 2)


def split_bits(nbits):
    cuts = [nbits * i // 4 for i in range(5)]
    return [list(range(cuts[i], cuts[i + 1])) for i in range(4)]


def orders_of(nbits, pieces):
    axes = split_bits(nbits)
    names = {"x": axes[0], "y": axes[1], "a": axes[2], "b": axes[3]}
    return [[b for name in ORDERS[p % len(ORDERS)] for b in names[name]] for p in range(pieces)]


def plan_of(nbits, pieces, halves):
    if nbits == 4 and pieces == len(ORDERS):
        return PLAN
    count = pieces // halves
    plan = []
    for g in range(count):
        plan += [("far", g)] + [("send", p) for p in range(g * halves, (g + 1) * halves)]
    plan += [("act", i) for i in range(4)] + [("grads", 0)]
    plan += [("near", g) for g in range(count)] + [("height", 0)]
    plan += [("taps", i) for i in range(TAP_CUTS)] + [("edge", 0), ("spread", 0)]
    for s in range(nbits):
        plan += [(p, s) for p in range(pieces)]
        if s == 0:
            plan += [("conv", i) for i in range(CONV_CUTS)] + [("cedge", 0)]
        if s == nbits - 2:
            plan += [("collect", 0)]
    return plan


def kernel(
    dims,
    cv_hbm, cg_hbm, co_hbm, taps_hbm, gain_hbm, shift_hbm, w_hbm, og_hbm,
    gv, gg, taps_out, gain_out, shift_out, proj_out,
    cv, cg, co, taps_ref, gain_ref, shift_ref, w, og, ogt, active, normed, dsilu, scaled, hgx, halo_out, halo_in,
    st_a, st_b, st_d, pk_a, pk_b, pk_c, pk_d, tapf, acc, sendbuf, recvbuf, tapacc, rowacc, flat, parts, mine, sent, whole,
    in_sem, tp_send, tp_recv, halo_send, halo_recv,
    rs_send, rs_recv, a_send, a_recv, b_send, b_recv, seen,
):
    n, nbits, groups, halves, chan_total = dims
    pieces = groups * halves
    rows, chan = co.shape
    width = og.shape[1]
    block = width // n
    part = block // halves
    gcols = chan // groups
    cblocks = chan // LANES
    gblocks = gcols // LANES
    ntaps = taps_ref.shape[0]
    reach = ntaps - 1
    halo = hgx.shape[1] - rows
    chunk = mine.shape[0]
    per = -(-(ntaps + 2) // 8) * 8
    me = lax.axis_index("sp")
    core = lax.axis_index("tp")
    other_core = 1 - core
    orders = orders_of(nbits, pieces)
    mybits = [bit(me, b) for b in range(nbits)]

    def partner(b):
        return me + (1 << b) * (1 - 2 * mybits[b])

    loads = [
        pltpu.make_async_copy(src, dst, in_sem.at[i])
        for i, (src, dst) in enumerate(
            (
                (co_hbm, co), (og_hbm, og), (w_hbm, w), (cg_hbm, cg), (cv_hbm, cv),
                (gain_hbm, gain_ref), (shift_hbm, shift_ref), (taps_hbm, taps_ref),
            )
        )
    ]
    loads[0].start()
    loads[5].start()
    loads[6].start()
    loads[1].start()

    barrier = pltpu.get_barrier_semaphore()

    def greet(device, c):
        pl.semaphore_signal(barrier, inc=1, device_id=(device, c), device_id_type=MESH)

    greet(me, other_core)
    for b in range(nbits):
        greet(partner(b), core)
    odd = mybits[0]
    beside = me - 1 + 2 * odd
    outside = jnp.where(odd == 1, me == n - 1, me == 0)

    @pl.when(jnp.logical_not(outside))
    def _():
        greet(beside, core)

    lane_low = lax.broadcasted_iota(jnp.int32, (1, LANES), 1) < LANES // 2
    nt = rows // LANES
    mid = LANES // 2

    def pack(dst):
        for t in range(nt):
            turned = st_a[t * LANES:(t + 1) * LANES, :].T
            dst[0, t:t + 1, :] = turned[:1, :]
            dst[1, t:t + 1, :] = turned[mid:mid + 1, :]

    def unpack(packed, dst):
        for t in range(nt):
            dst[t * LANES:(t + 1) * LANES, :] = jnp.broadcast_to(packed[t:t + 1, :], (LANES, LANES)).T

    def wide(x, count):
        return jnp.concatenate([x] * count, axis=1)

    loads[0].wait()
    for copy in loads[2:5] + loads[7:]:
        copy.start()

    def stats(i, carry):
        at = pl.ds(pl.multiple_of(i * 64, 64), 64)
        h = co[at, :].astype(F32)
        mean = jnp.sum(h, axis=1, keepdims=True) / chan
        d = h - mean
        m2 = jnp.sum(d * d, axis=1, keepdims=True)
        st_a[at, :] = jnp.where(lane_low, mean, m2)
        return carry

    repeat(0, rows // 64, stats, 2)
    pack(pk_a)
    pl.semaphore_wait(barrier, jnp.where(outside, nbits + 1, nbits + 2))
    swap_a = pltpu.make_async_remote_copy(
        src_ref=pk_a, dst_ref=pk_b, send_sem=tp_send.at[0], recv_sem=tp_recv.at[0],
        device_id=(me, other_core), device_id_type=MESH,
    )
    swap_a.start()

    def tell(b):
        pl.semaphore_signal(seen.at[b], inc=1, device_id=(partner(b), core), device_id_type=MESH)

    def heard(b):
        pl.semaphore_wait(seen.at[b], 1)
        if b + 2 < nbits:
            tell(b + 1)

    tell(0)
    loads[1].wait()
    sub = LANES // block

    def transpose(c, carry):
        t = og[:, pl.ds(pl.multiple_of(c * LANES, LANES), LANES)].T
        for s in range(sub):
            ogt[c * sub + s] = t[s * block:(s + 1) * block, :]
        return carry

    lax.fori_loop(0, width // LANES, transpose, 0)
    loads[5].wait()
    loads[6].wait()
    gain = gain_ref[...].reshape(1, chan)
    shift = shift_ref[...].reshape(1, chan)
    heard(0)
    swap_a.wait()
    gap = pk_a[0] - pk_b[0]
    variance = (pk_a[1] + pk_b[1] + gap * gap * (0.5 * chan)) / chan_total
    unpack(0.5 * (pk_a[0] + pk_b[0]), st_b)
    unpack(lax.rsqrt(variance + norm_eps), st_d)

    def norm_of(g):
        cols = slice(g * gcols, (g + 1) * gcols)

        def norm(i, carry):
            at = pl.ds(pl.multiple_of(i * 32, 32), 32)
            z = (co[at, cols].astype(F32) - wide(st_b[at, :], gblocks)) * wide(st_d[at, :], gblocks)
            normed[at, cols] = z
            x = z * gain[:, cols] + shift[:, cols]
            sig = jax.nn.sigmoid(x)
            active[at, cols] = (x * sig).astype(BF16)
            dsilu[at, cols] = sig * (1.0 + x * (1.0 - sig))
            return carry

        repeat(0, rows // 32, norm, 4)

    def stage_copy(p, k):
        count = n >> (k + 1)
        off = n - (n >> k)
        return pltpu.make_async_remote_copy(
            src_ref=sendbuf.at[p, pl.ds(off, count)],
            dst_ref=recvbuf.at[p, pl.ds(off, count)],
            send_sem=rs_send.at[p, k],
            recv_sem=rs_recv.at[p, k],
            device_id=(partner(orders[p][k]), core),
            device_id_type=MESH,
        )

    unit = max(1, min(n // 2, UNIT // part))

    def product(p, start):
        g, h = p // halves, p % halves
        found = []
        for i in range(unit):
            place = start + i
            owner = 0
            for k, b in enumerate(orders[p]):
                flip = place >> (nbits - 1 - k) & 1
                owner = owner + (1 - mybits[b] if flip else mybits[b]) * (1 << b)
            found.append(ogt[owner, h * part:(h + 1) * part, :])
        lhs = jnp.concatenate(found, axis=0)
        out = jnp.dot(lhs, active[:, g * gcols:(g + 1) * gcols], preferred_element_type=F32)
        return out.reshape(unit, part, gcols)

    def far(p):
        for i in range(0, n // 2, unit):
            sendbuf[p, i:i + unit] = product(p, n // 2 + i).astype(BF16)

    def near(p):
        for i in range(0, n // 2, unit):
            acc[p, i:i + unit] = product(p, i)

    def arrive(p, k):
        count = n >> (k + 1)
        off = n - (n >> k)
        stage_copy(p, k).wait_recv()
        if k + 1 < nbits:
            keep = count // 2

            def pass_on(i, carry):
                sendbuf[p, off + count + i] = (
                    acc[p, keep + i] + recvbuf[p, off + keep + i].astype(F32)
                ).astype(BF16)
                return carry

            lax.fori_loop(0, count - keep, pass_on, 0)
            stage_copy(p, k + 1).start()

            def take(i, carry):
                acc[p, i] = acc[p, i] + recvbuf[p, off + i].astype(F32)
                return carry

            lax.fori_loop(0, keep, take, 0)
        else:
            g, h = p // halves, p % halves
            proj_out[h * part:(h + 1) * part, g * gcols:(g + 1) * gcols] = (
                acc[p, 0] + recvbuf[p, off].astype(F32)
            )

    def act(i):
        count = rows // 4
        at = slice(i * count, (i + 1) * count)
        scaled[at, :] = jnp.dot(og[at, :], w[...], preferred_element_type=F32)

    def grads(i, carry):
        at = pl.ds(pl.multiple_of(i * 32, 32), 32)
        z = normed[at, :]
        ng = scaled[at, :] * dsilu[at, :]
        ngz = ng * z
        rowacc[0] = rowacc[0] + jnp.sum(ngz.reshape(4, 8, chan), axis=0)
        rowacc[1] = rowacc[1] + jnp.sum(ng.reshape(4, 8, chan), axis=0)
        s = ng * gain
        scaled[at, :] = s
        total = jnp.sum(s, axis=1, keepdims=True)
        dot = jnp.sum(s * z, axis=1, keepdims=True)
        st_a[at, :] = jnp.where(lane_low, total, dot)
        return carry

    def height(i, carry):
        at = pl.ds(pl.multiple_of(i * 32, 32), 32)
        hg = wide(st_d[at, :], cblocks) * (
            scaled[at, :] - wide(st_a[at, :], cblocks) - normed[at, :] * wide(st_b[at, :], cblocks)
        )
        for c in range(cblocks):
            hgx[c, at, :] = hg[:, c * LANES:(c + 1) * LANES]
        return carry

    halo_copy = pltpu.make_async_remote_copy(
        src_ref=halo_out, dst_ref=halo_in,
        send_sem=halo_send, recv_sem=halo_recv,
        device_id=(lax.rem(me + n - 1, n), core), device_id_type=MESH,
    )
    swap_b = pltpu.make_async_remote_copy(
        src_ref=pk_c, dst_ref=pk_d, send_sem=tp_send.at[1], recv_sem=tp_recv.at[1],
        device_id=(me, other_core), device_id_type=MESH,
    )
    step = 64
    steps = rows // step

    def tap_step(c, r):
        at = pl.ds(r, step)
        cols = pl.ds(pl.multiple_of(c * LANES, LANES), LANES)
        sig = jax.nn.sigmoid(cg[at, cols].astype(F32))
        gated = (cv[at, cols].astype(F32) * sig).astype(BF16).astype(F32)
        for j in range(ntaps):
            h = hgx[c, pl.ds(r + reach - j, step), :]
            tapacc[c, j] = tapacc[c, j] + jnp.sum((gated * h).reshape(step // 8, 8, LANES), axis=0)

    def taps_body(i, carry):
        tap_step(i // (steps - 1), pl.multiple_of(lax.rem(i, steps - 1) * step, step))
        return carry

    def taps_edge(c, carry):
        tap_step(c, rows - step)
        rowsum = jnp.sum(tapacc[c], axis=1)
        at = pl.ds(pl.multiple_of(c * per, 8), ntaps)
        flat[at, :] = rowsum
        return carry

    def conv_step(c, r):
        at = pl.ds(r, step)
        cols = pl.ds(pl.multiple_of(c * LANES, LANES), LANES)
        sig = jax.nn.sigmoid(cg[at, cols].astype(F32))
        value = cv[at, cols].astype(F32)
        total = jnp.zeros((step // 8, 8, LANES), F32)
        for j in range(ntaps):
            h = hgx[c, pl.ds(r + reach - j, step), :].reshape(step // 8, 8, LANES)
            total = total + tapf[c, j] * h
        total = total.reshape(step, LANES)
        gv[at, cols] = (total * sig).astype(BF16)
        gg[at, cols] = (total * value * sig * (1.0 - sig)).astype(BF16)

    def conv_body(i, carry):
        conv_step(i // (steps - 1), pl.multiple_of(lax.rem(i, steps - 1) * step, step))
        return carry

    def conv_edge(c, carry):
        conv_step(c, rows - step)
        return carry

    def peer_of(i):
        return lax.rem(me + i, n)

    def rows_of(device):
        return pl.ds(pl.multiple_of(device * chunk, chunk), chunk)

    def spread_copy(peer, slot):
        return pltpu.make_async_remote_copy(
            src_ref=flat.at[rows_of(peer)], dst_ref=parts.at[slot],
            send_sem=a_send.at[peer], recv_sem=a_recv.at[slot],
            device_id=(peer, core), device_id_type=MESH,
        )

    def collect_copy(peer, owner):
        return pltpu.make_async_remote_copy(
            src_ref=sent, dst_ref=whole.at[rows_of(owner)],
            send_sem=b_send.at[peer], recv_sem=b_recv.at[owner],
            device_id=(peer, core), device_id_type=MESH,
        )

    def loop(body):
        def run(i, carry):
            body(peer_of(i))
            return carry

        lax.fori_loop(1, n, run, 0)

    def add_part(peer):
        spread_copy(peer, peer).wait_recv()
        mine[...] = mine[...] + parts[peer]

    taps_total = cblocks * (steps - 1)
    for what, i in plan_of(nbits, pieces, halves):
        if what == "far":
            norm_of(i)
            for p in range(i * halves, (i + 1) * halves):
                far(p)
            if i == 0 and nbits > 2:
                heard(1)
        elif what == "send":
            stage_copy(i, 0).start()
        elif what == "near":
            for p in range(i * halves, (i + 1) * halves):
                near(p)
        elif what == "act":
            if i == 0:
                loads[2].wait()
                rowacc[...] = jnp.zeros_like(rowacc)
            act(i)
        elif what == "grads":
            repeat(0, rows // 32, grads, 2)
            pack(pk_c)
            swap_b.start()
            tapacc[...] = jnp.zeros_like(tapacc)
            loads[7].wait()
            for c in range(cblocks):
                for j in range(ntaps):
                    row = taps_ref[j:j + 1, c * LANES:(c + 1) * LANES].astype(F32)
                    tapf[c, j] = jnp.broadcast_to(row, (8, LANES))
            flat[...] = jnp.zeros_like(flat)
        elif what == "height":
            swap_b.wait()
            unpack((pk_c[0] + pk_d[0]) / chan_total, st_a)
            unpack((pk_c[1] + pk_d[1]) / chan_total, st_b)
            height(0, 0)
            halo_out[...] = hgx[:, :halo, :].astype(BF16)

            @pl.when(me > 0)
            def _():
                halo_copy.start()

            repeat(1, rows // 32, height, 3)
            loads[3].wait()
            loads[4].wait()
        elif what == "taps":
            lax.fori_loop(taps_total * i // TAP_CUTS, taps_total * (i + 1) // TAP_CUTS, taps_body, 0)
        elif what == "edge":
            @pl.when(me < n - 1)
            def _():
                halo_copy.wait_recv()

            hgx[:, rows:, :] = jnp.where(me < n - 1, halo_in[...].astype(F32), 0.0)
            lax.fori_loop(0, cblocks, taps_edge, 0)
            for c in range(cblocks):
                for j in range(2):
                    flat[c * per + ntaps + j:c * per + ntaps + j + 1, :] = jnp.sum(
                        rowacc[j, :, c * LANES:(c + 1) * LANES], axis=0, keepdims=True
                    )
        elif what == "spread":
            for b in range(2, nbits - 1):
                heard(b)
            loop(lambda peer: spread_copy(peer, me).start())
            mine[...] = flat[rows_of(me), :]
        elif what == "collect":
            loop(add_part)
            sent[...] = mine[...].astype(BF16)
            loop(lambda peer: collect_copy(peer, me).start())
            whole[rows_of(me), :] = sent[...]
        elif what == "conv":
            lax.fori_loop(taps_total * i // CONV_CUTS, taps_total * (i + 1) // CONV_CUTS, conv_body, 0)
        elif what == "cedge":
            lax.fori_loop(0, cblocks, conv_edge, 0)
        else:
            arrive(what, i)
    loop(lambda peer: collect_copy(peer, peer).wait_recv())
    for c in range(cblocks):
        cols = slice(c * LANES, (c + 1) * LANES)
        found = whole[c * per:(c + 1) * per, :].astype(F32)
        taps_out[:, cols] = found[:ntaps, :]
        gain_out[cols] = found[ntaps, :]
        shift_out[cols] = found[ntaps + 1, :]

    loop(lambda peer: spread_copy(peer, me).wait_send())
    loop(lambda peer: collect_copy(peer, me).wait_send())
    for p in range(pieces):
        for k in range(nbits):
            stage_copy(p, k).wait_send()

    @pl.when(me > 0)
    def _():
        halo_copy.wait_send()


def place(*refs):
    count = (len(refs) - 1) // 2
    sem = refs[-1]
    copies = [
        pltpu.make_async_copy(src, dst, sem.at[i])
        for i, (src, dst) in enumerate(zip(refs[:count], refs[count:-1]))
    ]
    for copy in copies:
        copy.start()
    for copy in copies:
        copy.wait()


def local(conv_value, conv_gate, conv_out, conv_taps, norm_gain, norm_shift, proj_weight, out_grad):
    rows, chan = conv_value.shape
    ntaps = conv_taps.shape[0]
    width = out_grad.shape[1]
    n = lax.axis_size("sp")
    nbits = n.bit_length() - 1
    assert 1 << nbits == n and lax.axis_size("tp") == 2
    groups = 3
    gcols = chan // groups
    block = width // n
    halves = min(HALVES, block // 8)
    pieces = groups * halves
    part = block // halves
    cblocks = chan // LANES
    halo = 32
    per = -(-(ntaps + 2) // 8) * 8
    chunk = -(-(-(-per * cblocks // n)) // 8) * 8
    dims = (n, nbits, groups, halves, chan * 2)
    hbm = pl.BlockSpec(memory_space=pl.ANY)
    vmem = pl.BlockSpec(memory_space=pltpu.VMEM)
    dma = pltpu.SemaphoreType.DMA
    results = pl.pallas_call(
        functools.partial(kernel, dims),
        out_shape=(
            pltpu.VMEM((rows, chan), BF16),
            pltpu.VMEM((rows, chan), BF16),
            pltpu.VMEM((ntaps, chan), F32),
            pltpu.VMEM((chan,), F32),
            pltpu.VMEM((chan,), F32),
            pltpu.VMEM((block, chan), F32),
        ),
        in_specs=[hbm] * 8,
        out_specs=(vmem,) * 6,
        scratch_shapes=[
            pltpu.VMEM((rows, chan), BF16),
            pltpu.VMEM((rows, chan), BF16),
            pltpu.VMEM((rows, chan), BF16),
            pltpu.VMEM((ntaps, chan), BF16),
            pltpu.VMEM((chan,), F32),
            pltpu.VMEM((chan,), F32),
            pltpu.VMEM((width, chan), BF16),
            pltpu.VMEM((rows, width), BF16),
            pltpu.VMEM((n, block, rows), BF16),
            pltpu.VMEM((rows, chan), BF16),
            pltpu.VMEM((rows, chan), F32),
            pltpu.VMEM((rows, chan), F32),
            pltpu.VMEM((rows, chan), F32),
            pltpu.VMEM((cblocks, rows + halo, LANES), F32),
            pltpu.VMEM((cblocks, halo, LANES), BF16),
            pltpu.VMEM((cblocks, halo, LANES), BF16),
            pltpu.VMEM((rows, LANES), F32),
            pltpu.VMEM((rows, LANES), F32),
            pltpu.VMEM((rows, LANES), F32),
            *[pltpu.VMEM((2, rows // LANES, LANES), F32)] * 4,
            pltpu.VMEM((cblocks, ntaps, 8, LANES), F32),
            pltpu.VMEM((pieces, n // 2, part, gcols), F32),
            pltpu.VMEM((pieces, n, part, gcols), BF16),
            pltpu.VMEM((pieces, n, part, gcols), BF16),
            pltpu.VMEM((cblocks, ntaps, 8, LANES), F32),
            pltpu.VMEM((2, 8, chan), F32),
            pltpu.VMEM((n * chunk, LANES), F32),
            pltpu.VMEM((n, chunk, LANES), F32),
            pltpu.VMEM((chunk, LANES), F32),
            pltpu.VMEM((chunk, LANES), BF16),
            pltpu.VMEM((n * chunk, LANES), BF16),
            dma((8,)),
            dma((2,)), dma((2,)),
            dma, dma,
            dma((pieces, nbits)), dma((pieces, nbits)),
            dma((n,)), dma((n,)),
            dma((n,)), dma((n,)),
            pltpu.SemaphoreType.REGULAR((nbits,)),
        ],
        compiler_params=pltpu.CompilerParams(
            collective_id=0, has_side_effects=True, vmem_limit_bytes=60 * 1024 * 1024
        ),
    )(
        conv_value, conv_gate, conv_out, conv_taps, norm_gain, norm_shift, proj_weight, out_grad,
    )
    return pl.pallas_call(
        place,
        out_shape=tuple(jax.ShapeDtypeStruct(x.shape, x.dtype) for x in results),
        in_specs=[vmem] * len(results),
        out_specs=(hbm,) * len(results),
        scratch_shapes=[dma((len(results),))],
    )(*[pltpu.with_memory_space_constraint(x, pltpu.VMEM) for x in results])


def solution(mesh):
    in_specs = (
        P("sp", "tp"),
        P("sp", "tp"),
        P("sp", "tp"),
        P(None, "tp"),
        P("tp"),
        P("tp"),
        P(None, "tp"),
        P("sp", None),
    )
    out_specs = (P("sp", "tp"), P("sp", "tp"), P(None, "tp"), P("tp"), P("tp"), P("sp", "tp"))
    return jax.shard_map(local, mesh=mesh, in_specs=in_specs, out_specs=out_specs, check_vma=False)
```

time: 53.8 us -> 45.1 us (0.84)
  Pallas kernels: 52.9 us -> 44.3 us
    pallas_call x1, Pallas kernels: 51.6 us -> 43 us  [local(): pl.pallas_call(functools.partial(kernel, dims), out_shape=(pltpu.VMEM((ro...]
where the time goes in v2:
time: 45.1 us; the launch traced here: 45 us
  Pallas kernels  44.3 us (98%)
  between operations  0.64 us (1%)
    pallas_call x1, Pallas kernels, local(): pl.pallas_call(functools.partial(kernel, dims), out_shape=(pltpu.VMEM((ro...  43 us
    pallas_call x1, Pallas kernels, local(): pl.pallas_call(place, out_shape=tuple((jax.ShapeDtypeStruct(x.shape, x.dt...  1.36 us

profile of v2, /device:TPU:0, one launch (start us, length us, event | category | flops | bytes accessed | tf_op | source)
XLA Modules:
  0.0 45.0 jit_solution(14073081142642702361)
XLA Ops:
  0.6 43.0 %shard_map.127 = (bf16[512,768]{1,0:T(8,128)(2,1)S(1)}, bf16[512,768]{1,0:T(8,128)(2,1)S(1)}, f32[31,768]{1,0:T(8,128)S(1)}, f32[768]{0:T(1024)S(1)}, f32[768]{0:T(1024)S(1)}, /*index=5*/f32[128,768]{1,0:T(8,128)S(1)}) custom-call(bf16[512,768]{1,0:T(8,128)(2,1)} %cv_hbm.1, bf16[512,768]{1,0:T(8,128)(2,1)} %cg_hbm.1, bf16[512,768]{1,0:T(8,128)(2,1)} %co_hbm.1, ...), custom_call_target="tpu_custom_call" | custom-call | tf_op jit(solution)/shard_map/pallas_call | solution.py:525
  43.6 1.4 %shard_map.128 = (bf16[512,768]{1,0:T(8,128)(2,1)}, bf16[512,768]{1,0:T(8,128)(2,1)}, f32[31,768]{1,0:T(8,128)}, f32[768]{0:T(1024)}, f32[768]{0:T(1024)}, /*index=5*/f32[128,768]{1,0:T(8,128)}) custom-call(bf16[512,768]{1,0:T(8,128)(2,1)S(1)} %get-tuple-element.12.refs_0_, bf16[512,768]{1,0:T(8,128)(2,1)S(1)} %get-tuple-element.13.refs_1_, ...), custom_call_target="tpu_custom_call" | custom-call | tf_op jit(solution)/shard_map/pallas_call | solution.py:583

commit v3 on v2

--- a/solution.py
+++ b/solution.py
@@ -16,17 +16,17 @@
 UNIT = 256
 TAP_CUTS = 6
 CONV_CUTS = 6
-ORDERS = ('ybax', 'xbya', 'byxa', 'xaby', 'xbya', 'xayb', 'yxab', 'ybxa', 'yxba', 'axyb', 'yxab', 'ayxb')
+ORDERS = ('xaby', 'yaxb', 'axby', 'yabx', 'xyab', 'yxab', 'yxab', 'axby', 'yaxb', 'xyab', 'xyab', 'abyx')
 PLAN = [
-    ("far", 0), ("send", 0), ("send", 2), ("send", 3), ("far", 1), ("send", 5), ("send", 7), ("far", 2), ("send", 8),
-    ("send", 11), ("act", 0), ("act", 1), ("act", 2), ("send", 4), ("send", 6), ("send", 9), ("act", 3), ("grads", 0),
-    ("near", 0), ("near", 1), (0, 0), (3, 0), ("near", 2), ("height", 0), ("send", 1), ("send", 10), ("taps", 0),
-    ("taps", 1), (5, 0), (7, 0), (11, 0), ("taps", 2), (2, 0), ("taps", 3), ("taps", 4), ("taps", 5), (4, 0), (8, 0),
-    (9, 0), ("conv", 0), ("conv", 1), (0, 1), ("edge", 0), (3, 1), (6, 0), ("spread", 0), ("conv", 2), (1, 0), (5, 1),
-    ("conv", 3), (8, 1), ("conv", 4), (10, 0), ("conv", 5), (7, 1), (9, 1), (11, 1), ("cedge", 0), (0, 2), (4, 1),
-    (6, 1), (2, 1), (3, 2), (5, 2), (10, 1), (9, 2), (7, 2), (4, 2), (11, 2), (3, 3), (1, 1), ("collect", 0), (0, 3),
-    (6, 2), (2, 2), (8, 2), (10, 2), (5, 3), (7, 3), (4, 3), (9, 3), (1, 2), (11, 3), (2, 3), (8, 3), (6, 3), (1, 3),
-    (10, 3),
+    ("far", 0), ("send", 0), ("send", 1), ("send", 2), ("send", 3), ("far", 1), ("send", 6), ("far", 2), ("send", 10),
+    ("send", 11), ("act", 0), ("act", 1), ("act", 2), ("send", 9), ("act", 3), ("grads", 0), ("send", 7), ("send", 8),
+    ("near", 0), (0, 0), (1, 0), (2, 0), ("near", 1), ("near", 2), ("height", 0), ("send", 4), ("send", 5),
+    ("taps", 0), ("taps", 1), (3, 0), (10, 0), (11, 0), ("taps", 2), ("taps", 3), ("taps", 4), ("taps", 5),
+    ("conv", 0), (6, 0), (7, 0), (9, 0), ("conv", 1), (0, 1), (2, 1), ("conv", 2), ("conv", 3), (1, 1), (8, 0),
+    ("conv", 4), ("edge", 0), (3, 1), ("spread", 0), ("conv", 5), (4, 0), (5, 0), ("cedge", 0), (11, 1), (6, 1),
+    (10, 1), (0, 2), (2, 2), (7, 1), (8, 1), (9, 1), (1, 2), (3, 2), (6, 2), (4, 1), (5, 1), (10, 2), (11, 2), (8, 2),
+    (0, 3), (2, 3), ("collect", 0), (3, 3), (9, 2), (7, 2), (1, 3), (11, 3), (4, 2), (6, 3), (5, 2), (7, 3), (10, 3),
+    (8, 3), (9, 3), (4, 3), (5, 3),
 ]
 
 
@@ -80,7 +80,7 @@
     cv_hbm, cg_hbm, co_hbm, taps_hbm, gain_hbm, shift_hbm, w_hbm, og_hbm,
     gv, gg, taps_out, gain_out, shift_out, proj_out,
     cv, cg, co, taps_ref, gain_ref, shift_ref, w, og, ogt, active, normed, dsilu, scaled, hgx, halo_out, halo_in,
-    st_a, st_b, st_d, pk_a, pk_b, pk_c, pk_d, tapf, acc, sendbuf, recvbuf, tapacc, rowacc, flat, parts, mine, sent, whole,
+    st_a, st_b, st_d, pk_a, pk_b, pk_c, pk_d, tapf, acc, sendbuf, recvbuf, tapacc, rowacc, flat, narrow, parts, mine, sent, whole,
     in_sem, tp_send, tp_recv, halo_send, halo_recv,
     rs_send, rs_recv, a_send, a_recv, b_send, b_recv, seen,
 ):
@@ -159,7 +159,7 @@
         copy.start()
 
     def stats(i, carry):
-        at = pl.ds(pl.multiple_of(i * 64, 64), 64)
+        at = pl.ds(pl.multiple_of(i * 32, 32), 32)
         h = co[at, :].astype(F32)
         mean = jnp.sum(h, axis=1, keepdims=True) / chan
         d = h - mean
@@ -167,7 +167,7 @@
         st_a[at, :] = jnp.where(lane_low, mean, m2)
         return carry
 
-    repeat(0, rows // 64, stats, 2)
+    repeat(0, rows // 32, stats, 8)
     pack(pk_a)
     pl.semaphore_wait(barrier, jnp.where(outside, nbits + 1, nbits + 2))
     swap_a = pltpu.make_async_remote_copy(
@@ -227,7 +227,7 @@
         return pltpu.make_async_remote_copy(
             src_ref=sendbuf.at[p, pl.ds(off, count)],
             dst_ref=recvbuf.at[p, pl.ds(off, count)],
-            send_sem=rs_send.at[p, k],
+            send_sem=rs_send,
             recv_sem=rs_recv.at[p, k],
             device_id=(partner(orders[p][k]), core),
             device_id_type=MESH,
@@ -373,15 +373,15 @@
 
     def spread_copy(peer, slot):
         return pltpu.make_async_remote_copy(
-            src_ref=flat.at[rows_of(peer)], dst_ref=parts.at[slot],
-            send_sem=a_send.at[peer], recv_sem=a_recv.at[slot],
+            src_ref=narrow.at[rows_of(peer)], dst_ref=parts.at[slot],
+            send_sem=a_send, recv_sem=a_recv,
             device_id=(peer, core), device_id_type=MESH,
         )
 
     def collect_copy(peer, owner):
         return pltpu.make_async_remote_copy(
             src_ref=sent, dst_ref=whole.at[rows_of(owner)],
-            send_sem=b_send.at[peer], recv_sem=b_recv.at[owner],
+            send_sem=b_send, recv_sem=b_recv,
             device_id=(peer, core), device_id_type=MESH,
         )
 
@@ -393,8 +393,17 @@
         lax.fori_loop(1, n, run, 0)
 
     def add_part(peer):
-        spread_copy(peer, peer).wait_recv()
-        mine[...] = mine[...] + parts[peer]
+        mine[...] = mine[...] + parts[peer].astype(F32)
+
+    def all_of(buffer, send_sem, recv_sem):
+        return pltpu.make_async_remote_copy(
+            src_ref=buffer, dst_ref=buffer, send_sem=send_sem, recv_sem=recv_sem,
+            device_id=(me, other_core), device_id_type=MESH,
+        )
+
+    all_parts = all_of(parts.at[pl.ds(0, n - 1)], a_send, a_recv)
+    all_whole = all_of(whole.at[pl.ds(0, (n - 1) * chunk)], b_send, b_recv)
+    all_pieces = all_of(sendbuf.at[:, pl.ds(0, n - 1)], rs_send, rs_recv.at[0, 0])
 
     taps_total = cblocks * (steps - 1)
     for what, i in plan_of(nbits, pieces, halves):
@@ -440,14 +449,14 @@
             loads[3].wait()
             loads[4].wait()
         elif what == "taps":
-            lax.fori_loop(taps_total * i // TAP_CUTS, taps_total * (i + 1) // TAP_CUTS, taps_body, 0)
+            lax.fori_loop(taps_total * i // TAP_CUTS, taps_total * (i + 1) // TAP_CUTS, taps_body, 0, unroll=7)
         elif what == "edge":
             @pl.when(me < n - 1)
             def _():
                 halo_copy.wait_recv()
 
             hgx[:, rows:, :] = jnp.where(me < n - 1, halo_in[...].astype(F32), 0.0)
-            lax.fori_loop(0, cblocks, taps_edge, 0)
+            lax.fori_loop(0, cblocks, taps_edge, 0, unroll=3)
             for c in range(cblocks):
                 for j in range(2):
                     flat[c * per + ntaps + j:c * per + ntaps + j + 1, :] = jnp.sum(
@@ -456,20 +465,22 @@
         elif what == "spread":
             for b in range(2, nbits - 1):
                 heard(b)
+            narrow[...] = flat[...].astype(BF16)
             loop(lambda peer: spread_copy(peer, me).start())
             mine[...] = flat[rows_of(me), :]
         elif what == "collect":
+            all_parts.wait_recv()
             loop(add_part)
             sent[...] = mine[...].astype(BF16)
             loop(lambda peer: collect_copy(peer, me).start())
             whole[rows_of(me), :] = sent[...]
         elif what == "conv":
-            lax.fori_loop(taps_total * i // CONV_CUTS, taps_total * (i + 1) // CONV_CUTS, conv_body, 0)
+            lax.fori_loop(taps_total * i // CONV_CUTS, taps_total * (i + 1) // CONV_CUTS, conv_body, 0, unroll=7)
         elif what == "cedge":
-            lax.fori_loop(0, cblocks, conv_edge, 0)
+            lax.fori_loop(0, cblocks, conv_edge, 0, unroll=3)
         else:
             arrive(what, i)
-    loop(lambda peer: collect_copy(peer, peer).wait_recv())
+    all_whole.wait_recv()
     for c in range(cblocks):
         cols = slice(c * LANES, (c + 1) * LANES)
         found = whole[c * per:(c + 1) * per, :].astype(F32)
@@ -477,11 +488,9 @@
         gain_out[cols] = found[ntaps, :]
         shift_out[cols] = found[ntaps + 1, :]
 
-    loop(lambda peer: spread_copy(peer, me).wait_send())
-    loop(lambda peer: collect_copy(peer, me).wait_send())
-    for p in range(pieces):
-        for k in range(nbits):
-            stage_copy(p, k).wait_send()
+    all_parts.wait_send()
+    all_whole.wait_send()
+    all_pieces.wait_send()
 
     @pl.when(me > 0)
     def _():
@@ -517,7 +526,7 @@
     cblocks = chan // LANES
     halo = 32
     per = -(-(ntaps + 2) // 8) * 8
-    chunk = -(-(-(-per * cblocks // n)) // 8) * 8
+    chunk = -(-(-(-per * cblocks // n)) // 16) * 16
     dims = (n, nbits, groups, halves, chan * 2)
     hbm = pl.BlockSpec(memory_space=pl.ANY)
     vmem = pl.BlockSpec(memory_space=pltpu.VMEM)
@@ -562,16 +571,17 @@
             pltpu.VMEM((cblocks, ntaps, 8, LANES), F32),
             pltpu.VMEM((2, 8, chan), F32),
             pltpu.VMEM((n * chunk, LANES), F32),
-            pltpu.VMEM((n, chunk, LANES), F32),
+            pltpu.VMEM((n * chunk, LANES), BF16),
+            pltpu.VMEM((n, chunk, LANES), BF16),
             pltpu.VMEM((chunk, LANES), F32),
             pltpu.VMEM((chunk, LANES), BF16),
             pltpu.VMEM((n * chunk, LANES), BF16),
             dma((8,)),
             dma((2,)), dma((2,)),
             dma, dma,
-            dma((pieces, nbits)), dma((pieces, nbits)),
-            dma((n,)), dma((n,)),
-            dma((n,)), dma((n,)),
+            dma, dma((pieces, nbits)),
+            dma, dma,
+            dma, dma,
             pltpu.SemaphoreType.REGULAR((nbits,)),
         ],
         compiler_params=pltpu.CompilerParams(

time: 45.1 us -> 41 us (0.909)
  Pallas kernels: 44.3 us -> 40.2 us
    pallas_call x1, Pallas kernels: 43 us -> 38.8 us  [local(): pl.pallas_call(functools.partial(kernel, dims), out_shape=(pltpu.VMEM((ro...]
where the time goes in v3:
time: 41 us; the launch traced here: 40.8 us
  Pallas kernels  40.2 us (98%)
  between operations  0.64 us (2%)
    pallas_call x1, Pallas kernels, local(): pl.pallas_call(functools.partial(kernel, dims), out_shape=(pltpu.VMEM((ro...  38.8 us
    pallas_call x1, Pallas kernels, local(): pl.pallas_call(place, out_shape=tuple((jax.ShapeDtypeStruct(x.shape, x.dt...  1.36 us

profile of v3, /device:TPU:0, one launch (start us, length us, event | category | flops | bytes accessed | tf_op | source)
XLA Modules:
  0.0 40.8 jit_solution(9729520575899007847)
XLA Ops:
  0.6 38.8 %shard_map.127 = (bf16[512,768]{1,0:T(8,128)(2,1)S(1)}, bf16[512,768]{1,0:T(8,128)(2,1)S(1)}, f32[31,768]{1,0:T(8,128)S(1)}, f32[768]{0:T(1024)S(1)}, f32[768]{0:T(1024)S(1)}, /*index=5*/f32[128,768]{1,0:T(8,128)S(1)}) custom-call(bf16[512,768]{1,0:T(8,128)(2,1)} %cv_hbm.1, bf16[512,768]{1,0:T(8,128)(2,1)} %cg_hbm.1, bf16[512,768]{1,0:T(8,128)(2,1)} %co_hbm.1, ...), custom_call_target="tpu_custom_call" | custom-call | tf_op jit(solution)/shard_map/pallas_call | solution.py:534
  39.5 1.4 %shard_map.128 = (bf16[512,768]{1,0:T(8,128)(2,1)}, bf16[512,768]{1,0:T(8,128)(2,1)}, f32[31,768]{1,0:T(8,128)}, f32[768]{0:T(1024)}, f32[768]{0:T(1024)}, /*index=5*/f32[128,768]{1,0:T(8,128)}) custom-call(bf16[512,768]{1,0:T(8,128)(2,1)S(1)} %get-tuple-element.12.refs_0_, bf16[512,768]{1,0:T(8,128)(2,1)S(1)} %get-tuple-element.13.refs_1_, ...), custom_call_target="tpu_custom_call" | custom-call | tf_op jit(solution)/shard_map/pallas_call | solution.py:593

commit v4 on v3

--- a/solution.py
+++ b/solution.py
@@ -16,17 +16,17 @@
 UNIT = 256
 TAP_CUTS = 6
 CONV_CUTS = 6
-ORDERS = ('xaby', 'yaxb', 'axby', 'yabx', 'xyab', 'yxab', 'yxab', 'axby', 'yaxb', 'xyab', 'xyab', 'abyx')
+ORDERS = ('byxa', 'yaxb', 'abyx', 'yxba', 'yxab', 'xyba', 'xbya', 'yabx', 'axyb', 'xayb', 'xayb', 'ybxa')
 PLAN = [
-    ("far", 0), ("send", 0), ("send", 1), ("send", 2), ("send", 3), ("far", 1), ("send", 6), ("far", 2), ("send", 10),
-    ("send", 11), ("act", 0), ("act", 1), ("act", 2), ("send", 9), ("act", 3), ("grads", 0), ("send", 7), ("send", 8),
-    ("near", 0), (0, 0), (1, 0), (2, 0), ("near", 1), ("near", 2), ("height", 0), ("send", 4), ("send", 5),
-    ("taps", 0), ("taps", 1), (3, 0), (10, 0), (11, 0), ("taps", 2), ("taps", 3), ("taps", 4), ("taps", 5),
-    ("conv", 0), (6, 0), (7, 0), (9, 0), ("conv", 1), (0, 1), (2, 1), ("conv", 2), ("conv", 3), (1, 1), (8, 0),
-    ("conv", 4), ("edge", 0), (3, 1), ("spread", 0), ("conv", 5), (4, 0), (5, 0), ("cedge", 0), (11, 1), (6, 1),
-    (10, 1), (0, 2), (2, 2), (7, 1), (8, 1), (9, 1), (1, 2), (3, 2), (6, 2), (4, 1), (5, 1), (10, 2), (11, 2), (8, 2),
-    (0, 3), (2, 3), ("collect", 0), (3, 3), (9, 2), (7, 2), (1, 3), (11, 3), (4, 2), (6, 3), (5, 2), (7, 3), (10, 3),
-    (8, 3), (9, 3), (4, 3), (5, 3),
+    ("far", 0), ("send", 0), ("send", 1), ("send", 2), ("far", 1), ("send", 7), ("send", 6), ("far", 2), ("send", 8),
+    ("act", 0), ("send", 5), ("act", 1), ("act", 2), ("send", 10), ("act", 3), ("send", 11), ("grads", 0),
+    ("near", 2), ("near", 0), ("near", 1), (1, 0), ("height", 0), (6, 0), ("taps", 0), ("conv", 0), ("send", 9),
+    ("taps", 1), ("send", 3), ("taps", 2), ("conv", 1), ("taps", 3), ("send", 4), (0, 0), (2, 0), (7, 0), ("taps", 4),
+    (8, 0), ("taps", 5), (11, 0), (10, 0), ("conv", 2), (5, 0), (1, 1), ("conv", 3), ("edge", 0), (3, 0),
+    ("spread", 0), (6, 1), (4, 0), (9, 0), (7, 1), (8, 1), (2, 1), ("conv", 4), ("conv", 5), (0, 1), (3, 1),
+    ("cedge", 0), (11, 1), (10, 1), (1, 2), (5, 1), (6, 2), (4, 1), (0, 2), (8, 2), (2, 2), ("collect", 0), (7, 2),
+    (9, 1), (10, 2), (11, 2), (6, 3), (3, 2), (9, 2), (2, 3), (4, 2), (5, 2), (8, 3), (1, 3), (0, 3), (3, 3), (10, 3),
+    (11, 3), (7, 3), (9, 3), (5, 3), (4, 3),
 ]
 
 
@@ -194,12 +194,11 @@
             ogt[c * sub + s] = t[s * block:(s + 1) * block, :]
         return carry
 
-    lax.fori_loop(0, width // LANES, transpose, 0)
+    lax.fori_loop(0, width // LANES, transpose, 0, unroll=4)
     loads[5].wait()
     loads[6].wait()
     gain = gain_ref[...].reshape(1, chan)
     shift = shift_ref[...].reshape(1, chan)
-    heard(0)
     swap_a.wait()
     gap = pk_a[0] - pk_b[0]
     variance = (pk_a[1] + pk_b[1] + gap * gap * (0.5 * chan)) / chan_total
@@ -411,8 +410,8 @@
             norm_of(i)
             for p in range(i * halves, (i + 1) * halves):
                 far(p)
-            if i == 0 and nbits > 2:
-                heard(1)
+            if i == 0:
+                heard(0)
         elif what == "send":
             stage_copy(i, 0).start()
         elif what == "near":
@@ -423,8 +422,10 @@
                 loads[2].wait()
                 rowacc[...] = jnp.zeros_like(rowacc)
             act(i)
+            if i == 0 and nbits > 2:
+                heard(1)
         elif what == "grads":
-            repeat(0, rows // 32, grads, 2)
+            repeat(0, rows // 32, grads, 4)
             pack(pk_c)
             swap_b.start()
             tapacc[...] = jnp.zeros_like(tapacc)

time: 41 us -> 40.1 us (0.978)
  Pallas kernels: 40.2 us -> 39.3 us
    pallas_call x1, Pallas kernels: 38.8 us -> 37.9 us  [local(): pl.pallas_call(functools.partial(kernel, dims), out_shape=(pltpu.VMEM((ro...]
where the time goes in v4:
time: 40.1 us; the launch traced here: 39.9 us
  Pallas kernels  39.3 us (98%)
  between operations  0.64 us (2%)
    pallas_call x1, Pallas kernels, local(): pl.pallas_call(functools.partial(kernel, dims), out_shape=(pltpu.VMEM((ro...  37.9 us
    pallas_call x1, Pallas kernels, local(): pl.pallas_call(place, out_shape=tuple((jax.ShapeDtypeStruct(x.shape, x.dt...  1.36 us

profile of v4, /device:TPU:0, one launch (start us, length us, event | category | flops | bytes accessed | tf_op | source)
XLA Modules:
  0.0 39.9 jit_solution(16408042828989532996)
XLA Ops:
  0.6 37.9 %shard_map.127 = (bf16[512,768]{1,0:T(8,128)(2,1)S(1)}, bf16[512,768]{1,0:T(8,128)(2,1)S(1)}, f32[31,768]{1,0:T(8,128)S(1)}, f32[768]{0:T(1024)S(1)}, f32[768]{0:T(1024)S(1)}, /*index=5*/f32[128,768]{1,0:T(8,128)S(1)}) custom-call(bf16[512,768]{1,0:T(8,128)(2,1)} %cv_hbm.1, bf16[512,768]{1,0:T(8,128)(2,1)} %cg_hbm.1, bf16[512,768]{1,0:T(8,128)(2,1)} %co_hbm.1, ...), custom_call_target="tpu_custom_call" | custom-call | tf_op jit(solution)/shard_map/pallas_call | solution.py:535
  38.6 1.4 %shard_map.128 = (bf16[512,768]{1,0:T(8,128)(2,1)}, bf16[512,768]{1,0:T(8,128)(2,1)}, f32[31,768]{1,0:T(8,128)}, f32[768]{0:T(1024)}, f32[768]{0:T(1024)}, /*index=5*/f32[128,768]{1,0:T(8,128)}) custom-call(bf16[512,768]{1,0:T(8,128)(2,1)S(1)} %get-tuple-element.12.refs_0_, bf16[512,768]{1,0:T(8,128)(2,1)S(1)} %get-tuple-element.13.refs_1_, ...), custom_call_target="tpu_custom_call" | custom-call | tf_op jit(solution)/shard_map/pallas_call | solution.py:594

commit v5 on v4

--- a/solution.py
+++ b/solution.py
@@ -159,7 +159,7 @@
         copy.start()
 
     def stats(i, carry):
-        at = pl.ds(pl.multiple_of(i * 32, 32), 32)
+        at = pl.ds(pl.multiple_of(i * 64, 64), 64)
         h = co[at, :].astype(F32)
         mean = jnp.sum(h, axis=1, keepdims=True) / chan
         d = h - mean
@@ -167,7 +167,7 @@
         st_a[at, :] = jnp.where(lane_low, mean, m2)
         return carry
 
-    repeat(0, rows // 32, stats, 8)
+    repeat(0, rows // 64, stats, 8)
     pack(pk_a)
     pl.semaphore_wait(barrier, jnp.where(outside, nbits + 1, nbits + 2))
     swap_a = pltpu.make_async_remote_copy(

time: 40.1 us -> 40 us (level)
  no operation moved by 1% of the time
where the time goes in v5:
time: 40 us; the launch traced here: 39.9 us
  Pallas kernels  39.2 us (98%)
  between operations  0.64 us (2%)
    pallas_call x1, Pallas kernels, local(): pl.pallas_call(functools.partial(kernel, dims), out_shape=(pltpu.VMEM((ro...  37.9 us
    pallas_call x1, Pallas kernels, local(): pl.pallas_call(place, out_shape=tuple((jax.ShapeDtypeStruct(x.shape, x.dt...  1.36 us

profile of v5, /device:TPU:0, one launch (start us, length us, event | category | flops | bytes accessed | tf_op | source)
XLA Modules:
  0.0 39.9 jit_solution(10389932388916926629)
XLA Ops:
  0.6 37.9 %shard_map.127 = (bf16[512,768]{1,0:T(8,128)(2,1)S(1)}, bf16[512,768]{1,0:T(8,128)(2,1)S(1)}, f32[31,768]{1,0:T(8,128)S(1)}, f32[768]{0:T(1024)S(1)}, f32[768]{0:T(1024)S(1)}, /*index=5*/f32[128,768]{1,0:T(8,128)S(1)}) custom-call(bf16[512,768]{1,0:T(8,128)(2,1)} %cv_hbm.1, bf16[512,768]{1,0:T(8,128)(2,1)} %cg_hbm.1, bf16[512,768]{1,0:T(8,128)(2,1)} %co_hbm.1, ...), custom_call_target="tpu_custom_call" | custom-call | tf_op jit(solution)/shard_map/pallas_call | solution.py:535
  38.5 1.4 %shard_map.128 = (bf16[512,768]{1,0:T(8,128)(2,1)}, bf16[512,768]{1,0:T(8,128)(2,1)}, f32[31,768]{1,0:T(8,128)}, f32[768]{0:T(1024)}, f32[768]{0:T(1024)}, /*index=5*/f32[128,768]{1,0:T(8,128)}) custom-call(bf16[512,768]{1,0:T(8,128)(2,1)S(1)} %get-tuple-element.12.refs_0_, bf16[512,768]{1,0:T(8,128)(2,1)S(1)} %get-tuple-element.13.refs_1_, ...), custom_call_target="tpu_custom_call" | custom-call | tf_op jit(solution)/shard_map/pallas_call | solution.py:594
